TPU v7x, 32 devices: a whole 2x2x4 slice. The times are simulated.
32 devices in a mesh: fs: 4 (over z), tp: 4 (over y, x), rep: 2 (over core).
Axes of the slice: x: 2, y: 2, z: 4, core: 2. Of those that a mesh axis runs over, the one named last changes fastest.
Arguments:
- up_weight: float32 [2048, 8192], P('fs', ('tp', 'rep')), may hold values from -0.125 to 0.125
- up_momentum: float32 [2048, 8192], P('fs', ('tp', 'rep')), may hold values from -24 to 24
- up_grads: bfloat16 [2, 2048, 8192], P('rep', 'fs', 'tp'), may hold values from -2.09375 to 2.09375
- out_weight: float32 [2048, 2048], P('fs', ('tp', 'rep')), may hold values from -0.125 to 0.125
- out_momentum: float32 [2048, 2048], P('fs', ('tp', 'rep')), may hold values from -24 to 24
- out_grads: bfloat16 [2, 2048, 2048], P('rep', 'fs', 'tp'), may hold values from -2.09375 to 2.09375
Outputs:
- up_weight_new: float32 [2048, 8192], P('fs', ('tp', 'rep'))
- up_momentum_new: float32 [2048, 8192], P('fs', ('tp', 'rep'))
- up_direction: float32 [2048, 8192], P('fs', ('tp', 'rep'))
- out_weight_new: float32 [2048, 2048], P('fs', ('tp', 'rep'))
- out_momentum_new: float32 [2048, 2048], P('fs', ('tp', 'rep'))
- out_direction: float32 [2048, 2048], P('fs', ('tp', 'rep'))
All inputs are finite; a program needn't handle non-finite values.
Results may differ from a plain program's by a relative error of at most 0.039.
Values may be sent and summed in bfloat16 or wider, within the bound.
No kernel may reach another device: no remote copies, remote signals or barrier semaphores. Data moves between devices by JAX's collectives and lax.ppermute only.
A program may use at most 64 MiB of HBM per device.

v0:
```python
import math
import jax
import jax.numpy as jnp
from jax import lax
from jax.sharding import PartitionSpec as P

ITERS = 3
MOMENT = 0.9
RATE = 0.02
COEF_A = 3.4445
COEF_B = -4.775
COEF_C = 2.0315


def local_gram(values, columns):
    return lax.dot_general(
        values, columns, (((1,), (1,)), ((), ())), preferred_element_type=jnp.float32
    )


def contract(gram, values, gram_axis):
    return lax.dot_general(
        gram, values, (((gram_axis,), (0,)), ((), ())), preferred_element_type=jnp.float32
    )


def second_product(gram, first_half, gram_axis):
    return contract(gram, lax.all_gather(first_half, "fs", axis=0, tiled=True), gram_axis)


def on_device(up_weight, up_momentum, up_grads, out_weight, out_momentum, out_grads):
    grad_up, grad_out = (
        lax.psum_scatter(
            up_grads[0].astype(jnp.float32).astype(jnp.bfloat16),
            "rep",
            scatter_dimension=1,
            tiled=True,
        ).astype(jnp.float32),
        lax.psum_scatter(
            out_grads[0].astype(jnp.float32).astype(jnp.bfloat16),
            "rep",
            scatter_dimension=1,
            tiled=True,
        ).astype(jnp.float32),
    )
    moments = [MOMENT * up_momentum + grad_up, MOMENT * out_momentum + grad_out]
    group = lax.axis_size("tp") * lax.axis_size("rep")
    current = moments
    for iteration in range(ITERS):
        values = [entry.astype(jnp.bfloat16) for entry in current]
        columns = (
            lax.all_gather(values[0], "fs", axis=0, tiled=True),
            lax.all_gather(values[1], "fs", axis=0, tiled=True),
        )
        gram_sums = (
            lax.psum(local_gram(values[0], columns[0]).astype(jnp.bfloat16), ("tp", "rep")).astype(
                jnp.float32
            ),
            lax.psum(local_gram(values[1], columns[1]).astype(jnp.bfloat16), ("tp", "rep")).astype(
                jnp.float32
            ),
        )
        gram_axis = 1
        if iteration == 0:
            totals = lax.psum(
                (jnp.sum(gram_sums[0] * gram_sums[0]), jnp.sum(gram_sums[1] * gram_sums[1])), "fs"
            )
        if iteration == 0:
            squares = [1.0 / (jnp.sqrt(total) + 1.0) for total in totals]
            factors = [jnp.sqrt(square) for square in squares]
        else:
            squares = [1.0, 1.0]
            factors = [1.0, 1.0]
        halves = [(gram_sums[index] * squares[index]).astype(jnp.bfloat16) for index in range(2)]
        products = [
            factors[index] * contract(halves[index], columns[index], gram_axis)
            for index in range(2)
        ]
        seconds = [
            second_product(halves[index], products[index].astype(jnp.bfloat16), gram_axis)
            for index in range(2)
        ]
        current = [
            COEF_A * factors[index] * current[index]
            + COEF_B * products[index]
            + COEF_C * seconds[index]
            for index in range(2)
        ]
    widths = [up_weight.shape[1] * group, out_weight.shape[1] * group]
    directions = [current[index] * math.sqrt(widths[index]) for index in range(2)]
    return (
        up_weight - RATE * directions[0],
        moments[0],
        directions[0],
        out_weight - RATE * directions[1],
        moments[1],
        directions[1],
    )


def solution(mesh):
    return jax.shard_map(
        on_device,
        mesh=mesh,
        in_specs=(
            P("fs", ("tp", "rep")),
            P("fs", ("tp", "rep")),
            P("rep", "fs", "tp"),
            P("fs", ("tp", "rep")),
            P("fs", ("tp", "rep")),
            P("rep", "fs", "tp"),
        ),
        out_specs=(
            P("fs", ("tp", "rep")),
            P("fs", ("tp", "rep")),
            P("fs", ("tp", "rep")),
            P("fs", ("tp", "rep")),
            P("fs", ("tp", "rep")),
            P("fs", ("tp", "rep")),
        ),
        check_vma=False,
    )
```

profile of v0, /device:TPU:0, one launch (start us, length us, event | category | flops | bytes accessed | tf_op | source)
XLA Modules:
  0.0 994.7 jit_solution(5314064352922162735)
XLA Ops:
  7.2 0.0 reduce-scatter.5.cloned.1.call-start
  7.2 0.7 reduce-scatter.5.cloned.1.call-update
  7.9 0.0 reduce-scatter.3.cloned.1.call-start
  8.0 0.7 reduce-scatter.3.cloned.1.call-update
  8.7 0.0 all-gather.25.cloned.1.call-start
  8.7 12.2 %reduce-scatter.5.cloned.1.call-done = bf16[512,256]{1,0:T(8,128)(2,1)} async-done(((bf16[512,512]{1,0:T(8,128)(2,1)}), bf16[512,256]{1,0:T(8,128)(2,1)}) %reduce-scatter.5.cloned.1.call-update) | async-done | bytes 262160 | tf_op jit(solution)/shard_map/reduce_scatter | solution.py:39
  20.9 1.9 fusion.25
  22.8 0.0 all-gather.25.cloned.1.call-update
  22.8 0.0 all-gather.13.cloned.1.call-start
  22.9 11.0 %reduce-scatter.3.cloned.1.call-done = bf16[512,1024]{1,0:T(8,128)(2,1)} async-done(((bf16[512,2048]{1,0:T(8,128)(2,1)}), bf16[512,1024]{1,0:T(8,128)(2,1)}) %reduce-scatter.3.cloned.1.call-update) | async-done | bytes 1048592 | tf_op jit(solution)/shard_map/reduce_scatter | solution.py:33
  33.9 3.3 fusion.26
  37.2 0.0 all-gather.13.cloned.1.call-update
  37.3 0.0 all-reduce.12.cloned.1.call-start
  37.3 28.1 %all-gather.25.cloned.1.call-done = bf16[2048,256]{1,0:T(8,128)(2,1)} async-done(((bf16[512,256]{1,0:T(8,128)(2,1)}), bf16[2048,256]{1,0:T(8,128)(2,1)}) %all-gather.25.cloned.1.call-update) | async-done | bytes 1048592 | tf_op jit(solution)/shard_map/all_gather | solution.py:53
  65.4 3.3 convolution_convert_fusion.2
  68.7 78.9 %all-gather.13.cloned.1.call-done = bf16[2048,1024]{1,0:T(8,128)(2,1)} async-done(((bf16[512,1024]{1,0:T(8,128)(2,1)}), bf16[2048,1024]{1,0:T(8,128)(2,1)}) %all-gather.13.cloned.1.call-update) | async-done | bytes 4194320 | tf_op jit(solution)/shard_map/all_gather | solution.py:52
  147.5 5.9 convolution_convert_fusion.5
  153.4 0.0 all-gather.27.cloned.1.call-start
  153.5 79.4 %all-reduce.12.cloned.1.call-done = (bf16[512,2048]{1,0:T(8,128)(2,1)}, bf16[512,2048]{1,0:T(8,128)(2,1)}) async-done(((bf16[512,2048]{1,0:T(8,128)(2,1)}, bf16[512,2048]{1,0:T(8,128)(2,1)}), (bf16[512,2048]{1,0:T(8,128)(2,1)}, bf16[512,2048]{1,0:T(8,128)(2,1)})) %all-reduce.12.cloned.1.call-update) | async-done | bytes 4194320 | tf_op jit(solution)/shard_map/psum | solution.py:56
  232.9 4.0 fusion
  236.9 12.3 %all-reduce = (f32[]{:T(128)}, f32[]{:T(128)}) all-reduce(f32[]{:T(128)} %get-tuple-element.42, f32[]{:T(128)} %get-tuple-element.43), channel_id=1, replica_groups=mesh['fs'=4,'tp'=4,'rep'=2] {'fs'}, use_global_device_ids=true, to_apply=%region_3.0 | all-reduce | flops 2 | bytes 16 | tf_op jit(solution)/shard_map/psum | solution.py:65
  250.0 3.3 fusion.28
  253.3 0.0 all-gather.27.cloned.1.call-update
  253.4 0.0 all-gather.15.cloned.1.call-start
  254.2 6.3 multiply_convert_fusion
  260.5 0.0 all-gather.15.cloned.1.call-update
  260.5 0.0 all-gather.29.cloned.1.call-start
  260.6 18.3 %all-gather.27.cloned.1.call-done = bf16[2048,256]{1,0:T(8,128)(2,1)} async-done(((bf16[512,256]{1,0:T(8,128)(2,1)}), bf16[2048,256]{1,0:T(8,128)(2,1)}) %all-gather.27.cloned.1.call-update) | async-done | bytes 1048592 | tf_op jit(solution)/shard_map/all_gather | solution.py:28
  278.8 3.6 fusion.29
  282.5 0.0 all-gather.17.cloned.1.call-start
  282.5 78.6 %all-gather.15.cloned.1.call-done = bf16[2048,1024]{1,0:T(8,128)(2,1)} async-done(((bf16[512,1024]{1,0:T(8,128)(2,1)}), bf16[2048,1024]{1,0:T(8,128)(2,1)}) %all-gather.15.cloned.1.call-update) | async-done | bytes 4194320 | tf_op jit(solution)/shard_map/all_gather | solution.py:28
  361.1 7.6 fusion.27
  368.7 0.0 all-gather.17.cloned.1.call-update
  368.7 0.2 all-reduce.10.cloned.1.call-start
  369.0 20.8 %all-gather.29.cloned.1.call-done = bf16[2048,256]{1,0:T(8,128)(2,1)} async-done(((bf16[512,256]{1,0:T(8,128)(2,1)}), bf16[2048,256]{1,0:T(8,128)(2,1)}) %all-gather.29.cloned.1.call-update) | async-done | bytes 1048592 | tf_op jit(solution)/shard_map/all_gather | solution.py:53
  389.8 3.3 convolution_convert_fusion.1
  393.1 79.0 %all-gather.17.cloned.1.call-done = bf16[2048,1024]{1,0:T(8,128)(2,1)} async-done(((bf16[512,1024]{1,0:T(8,128)(2,1)}), bf16[2048,1024]{1,0:T(8,128)(2,1)}) %all-gather.17.cloned.1.call-update) | async-done | bytes 4194320 | tf_op jit(solution)/shard_map/all_gather | solution.py:52
  472.1 5.9 convolution_convert_fusion.4
  478.0 0.0 all-reduce.10.cloned.1.call-update
  478.0 0.0 all-gather.31.cloned.1.call-start
  478.0 79.4 %all-reduce.10.cloned.1.call-done = (bf16[512,2048]{1,0:T(8,128)(2,1)}, bf16[512,2048]{1,0:T(8,128)(2,1)}) async-done(((bf16[512,2048]{1,0:T(8,128)(2,1)}, bf16[512,2048]{1,0:T(8,128)(2,1)}), (bf16[512,2048]{1,0:T(8,128)(2,1)}, bf16[512,2048]{1,0:T(8,128)(2,1)})) %all-reduce.10.cloned.1.call-update) | async-done | bytes 4194320 | tf_op jit(solution)/shard_map/psum | solution.py:56
  557.5 3.0 fusion.32
  560.5 0.0 all-gather.19.cloned.1.call-start
  560.6 6.9 fusion.30
  567.5 0.0 all-gather.33.cloned.1.call-start
  567.6 21.1 %all-gather.31.cloned.1.call-done = bf16[2048,256]{1,0:T(8,128)(2,1)} async-done(((bf16[512,256]{1,0:T(8,128)(2,1)}), bf16[2048,256]{1,0:T(8,128)(2,1)}) %all-gather.31.cloned.1.call-update) | async-done | bytes 1048592 | tf_op jit(solution)/shard_map/all_gather | solution.py:28
  588.7 2.8 fusion.33
  591.5 0.0 all-gather.21.cloned.1.call-start
  591.6 78.7 %all-gather.19.cloned.1.call-done = bf16[2048,1024]{1,0:T(8,128)(2,1)} async-done(((bf16[512,1024]{1,0:T(8,128)(2,1)}), bf16[2048,1024]{1,0:T(8,128)(2,1)}) %all-gather.19.cloned.1.call-update) | async-done | bytes 4194320 | tf_op jit(solution)/shard_map/all_gather | solution.py:28
  670.3 8.4 fusion.31
  678.6 0.0 all-reduce.8.cloned.1.call-start
  678.7 20.2 %all-gather.33.cloned.1.call-done = bf16[2048,256]{1,0:T(8,128)(2,1)} async-done(((bf16[512,256]{1,0:T(8,128)(2,1)}), bf16[2048,256]{1,0:T(8,128)(2,1)}) %all-gather.33.cloned.1.call-update) | async-done | bytes 1048592 | tf_op jit(solution)/shard_map/all_gather | solution.py:53
  698.9 3.3 convolution_convert_fusion
  702.2 78.3 %all-gather.21.cloned.1.call-done = bf16[2048,1024]{1,0:T(8,128)(2,1)} async-done(((bf16[512,1024]{1,0:T(8,128)(2,1)}), bf16[2048,1024]{1,0:T(8,128)(2,1)}) %all-gather.21.cloned.1.call-update) | async-done | bytes 4194320 | tf_op jit(solution)/shard_map/all_gather | solution.py:52
  780.5 5.9 convolution_convert_fusion.3
  786.4 0.0 all-gather.35.cloned.1.call-start
  786.4 79.4 %all-reduce.8.cloned.1.call-done = (bf16[512,2048]{1,0:T(8,128)(2,1)}, bf16[512,2048]{1,0:T(8,128)(2,1)}) async-done(((bf16[512,2048]{1,0:T(8,128)(2,1)}, bf16[512,2048]{1,0:T(8,128)(2,1)}), (bf16[512,2048]{1,0:T(8,128)(2,1)}, bf16[512,2048]{1,0:T(8,128)(2,1)})) %all-reduce.8.cloned.1.call-update) | async-done | bytes 4194320 | tf_op jit(solution)/shard_map/psum | solution.py:56
  865.9 3.0 fusion.35
  868.9 0.3 all-gather.23.cloned.1.call-start
  869.2 7.0 fusion.34
  876.2 20.9 %all-gather.35.cloned.1.call-done = bf16[2048,256]{1,0:T(8,128)(2,1)} async-done(((bf16[512,256]{1,0:T(8,128)(2,1)}), bf16[2048,256]{1,0:T(8,128)(2,1)}) %all-gather.35.cloned.1.call-update) | async-done | bytes 1048592 | tf_op jit(solution)/shard_map/all_gather | solution.py:28
  897.1 3.1 broadcast_multiply_fusion.1
  900.2 78.5 %all-gather.23.cloned.1.call-done = bf16[2048,1024]{1,0:T(8,128)(2,1)} async-done(((bf16[512,1024]{1,0:T(8,128)(2,1)}), bf16[2048,1024]{1,0:T(8,128)(2,1)}) %all-gather.23.cloned.1.call-update) | async-done | bytes 4194320 | tf_op jit(solution)/shard_map/all_gather | solution.py:28
  978.7 9.5 broadcast_multiply_fusion
  (43 shorter events, 0.2 us)
Async XLA Ops:
  7.2 13.7 %copy-start.14 = (f32[512,256]{1,0:T(8,128)S(1)}, f32[512,256]{1,0:T(8,128)}, u32[]{:S(2)}) copy-start(f32[512,256]{1,0:T(8,128)} %param.10) | copy-start | bytes 1572868
  7.2 13.7 %reduce-scatter.5.cloned.1.call-start = ((), (), s32[]{:S(2)}) async-start(), calls=%async_computation.9 | async-start | bytes 786432 | tf_op jit(solution)/shard_map/reduce_scatter | solution.py:39
  7.9 26.0 %copy-start.7 = (f32[512,1024]{1,0:T(8,128)S(1)}, f32[512,1024]{1,0:T(8,128)}, u32[]{:S(2)}) copy-start(f32[512,1024]{1,0:T(8,128)} %param.7) | copy-start | bytes 6291460
  7.9 26.0 %reduce-scatter.3.cloned.1.call-start = ((), (), s32[]{:S(2)}) async-start(), calls=%async_computation.2 | async-start | bytes 3145728 | tf_op jit(solution)/shard_map/reduce_scatter | solution.py:33
  8.7 56.7 %all-gather.25.cloned.1.call-start = ((), (), s32[]{:S(2)}) async-start(), calls=%async_computation.10 | async-start | bytes 1310720 | tf_op jit(solution)/shard_map/all_gather | solution.py:53
  22.8 42.6 %copy-start.6 = (bf16[512,256]{1,0:T(8,128)(2,1)S(1)}, bf16[512,256]{1,0:T(8,128)(2,1)}, u32[]{:S(2)}) copy-start(bf16[512,256]{1,0:T(8,128)(2,1)} %get-tuple-element.14) | copy-start | bytes 786436
  22.8 124.7 %all-gather.13.cloned.1.call-start = ((), (), s32[]{:S(2)}) async-start(), calls=%async_computation.3 | async-start | bytes 5242880 | tf_op jit(solution)/shard_map/all_gather | solution.py:52
  37.2 110.3 %copy-start.4 = (bf16[512,1024]{1,0:T(8,128)(2,1)S(1)}, bf16[512,1024]{1,0:T(8,128)(2,1)}, u32[]{:S(2)}) copy-start(bf16[512,1024]{1,0:T(8,128)(2,1)} %get-tuple-element.16) | copy-start | bytes 3145732
  37.3 195.7 %all-reduce.12.cloned.1.call-start = ((), (), s32[]{:S(2)}) async-start(), calls=%async_computation.18 | async-start | bytes 8388608 | tf_op jit(solution)/shard_map/psum | solution.py:56
  153.4 125.4 %all-gather.27.cloned.1.call-start = ((), (), s32[]{:S(2)}) async-start(), calls=%async_computation.11 | async-start | bytes 1310720 | tf_op jit(solution)/shard_map/all_gather | solution.py:28
  232.9 17.1 %copy-start.10 = (bf16[2048,256]{1,0:T(8,128)(2,1)S(1)}, bf16[2048,256]{1,0:T(8,128)(2,1)}, u32[]{:S(2)}) copy-start(bf16[2048,256]{1,0:T(8,128)(2,1)} %all-gather.25.cloned.1.call-done) | copy-start | bytes 3145732
  250.0 4.2 copy-start.9
  253.4 107.8 %all-gather.15.cloned.1.call-start = ((), (), s32[]{:S(2)}) async-start(), calls=%async_computation.4 | async-start | bytes 5242880 | tf_op jit(solution)/shard_map/all_gather | solution.py:28
  254.2 24.7 %copy-start.15 = (f32[512,256]{1,0:T(8,128)S(1)}, f32[512,256]{1,0:T(8,128)}, u32[]{:S(2)}) copy-start(f32[512,256]{1,0:T(8,128)} %get-tuple-element.15) | copy-start | bytes 1572868
  254.2 24.6 %copy-start.16 = (f32[512,256]{1,0:T(8,128)S(1)}, f32[512,256]{1,0:T(8,128)}, u32[]{:S(2)}) copy-start(f32[512,256]{1,0:T(8,128)} %get-tuple-element.27) | copy-start | bytes 1572868
  260.5 129.3 %all-gather.29.cloned.1.call-start = ((), (), s32[]{:S(2)}) async-start(), calls=%async_computation.12 | async-start | bytes 1310720 | tf_op jit(solution)/shard_map/all_gather | solution.py:53
  278.8 82.3 %copy-start.8 = (f32[512,1024]{1,0:T(8,128)S(1)}, f32[512,1024]{1,0:T(8,128)}, u32[]{:S(2)}) copy-start(f32[512,1024]{1,0:T(8,128)} %get-tuple-element.17) | copy-start | bytes 6291460
  282.5 189.6 %all-gather.17.cloned.1.call-start = ((), (), s32[]{:S(2)}) async-start(), calls=%async_computation.5 | async-start | bytes 5242880 | tf_op jit(solution)/shard_map/all_gather | solution.py:52
  361.1 28.6 %copy-start.13 = (bf16[512,256]{1,0:T(8,128)(2,1)S(1)}, bf16[512,256]{1,0:T(8,128)(2,1)}, u32[]{:S(2)}) copy-start(bf16[512,256]{1,0:T(8,128)(2,1)} %get-tuple-element.28) | copy-start | bytes 786436
  368.7 103.4 %copy-start.11 = (bf16[512,1024]{1,0:T(8,128)(2,1)S(1)}, bf16[512,1024]{1,0:T(8,128)(2,1)}, u32[]{:S(2)}) copy-start(bf16[512,1024]{1,0:T(8,128)(2,1)} %get-tuple-element.24) | copy-start | bytes 3145732
  368.7 188.7 %all-reduce.10.cloned.1.call-start = ((), (), s32[]{:S(2)}) async-start(), calls=%async_computation.17 | async-start | bytes 8388608 | tf_op jit(solution)/shard_map/psum | solution.py:56
  477.9 79.5 %copy-start.2 = (bf16[2048,256]{1,0:T(8,128)(2,1)S(1)}, bf16[2048,256]{1,0:T(8,128)(2,1)}, u32[]{:S(2)}) copy-start(bf16[2048,256]{1,0:T(8,128)(2,1)} %all-gather.29.cloned.1.call-done) | copy-start | bytes 3145732
  478.0 110.7 %all-gather.31.cloned.1.call-start = ((), (), s32[]{:S(2)}) async-start(), calls=%async_computation.13 | async-start | bytes 1310720 | tf_op jit(solution)/shard_map/all_gather | solution.py:28
  560.5 109.8 %all-gather.19.cloned.1.call-start = ((), (), s32[]{:S(2)}) async-start(), calls=%async_computation.6 | async-start | bytes 5242880 | tf_op jit(solution)/shard_map/all_gather | solution.py:28
  560.5 28.2 %copy-start = (bf16[512,2048]{1,0:T(8,128)(2,1)S(1)}, bf16[512,2048]{1,0:T(8,128)(2,1)}, u32[]{:S(2)}) copy-start(bf16[512,2048]{1,0:T(8,128)(2,1)} %get-tuple-element.11) | copy-start | bytes 6291460
  567.5 131.4 %all-gather.33.cloned.1.call-start = ((), (), s32[]{:S(2)}) async-start(), calls=%async_computation.14 | async-start | bytes 1310720 | tf_op jit(solution)/shard_map/all_gather | solution.py:53
  591.5 189.0 %all-gather.21.cloned.1.call-start = ((), (), s32[]{:S(2)}) async-start(), calls=%async_computation.7 | async-start | bytes 5242880 | tf_op jit(solution)/shard_map/all_gather | solution.py:52
  670.3 28.6 %copy-start.5 = (bf16[512,256]{1,0:T(8,128)(2,1)S(1)}, bf16[512,256]{1,0:T(8,128)(2,1)}, u32[]{:S(2)}) copy-start(bf16[512,256]{1,0:T(8,128)(2,1)} %get-tuple-element.36) | copy-start | bytes 786436
  678.6 101.9 %copy-start.12 = (bf16[512,1024]{1,0:T(8,128)(2,1)S(1)}, bf16[512,1024]{1,0:T(8,128)(2,1)}, u32[]{:S(2)}) copy-start(bf16[512,1024]{1,0:T(8,128)(2,1)} %get-tuple-element.32) | copy-start | bytes 3145732
  678.6 187.2 %all-reduce.8.cloned.1.call-start = ((), (), s32[]{:S(2)}) async-start(), calls=%async_computation.16 | async-start | bytes 8388608 | tf_op jit(solution)/shard_map/psum | solution.py:56
  786.4 79.5 %copy-start.3 = (bf16[2048,256]{1,0:T(8,128)(2,1)S(1)}, bf16[2048,256]{1,0:T(8,128)(2,1)}, u32[]{:S(2)}) copy-start(bf16[2048,256]{1,0:T(8,128)(2,1)} %all-gather.33.cloned.1.call-done) | copy-start | bytes 3145732
  786.4 110.7 %all-gather.35.cloned.1.call-start = ((), (), s32[]{:S(2)}) async-start(), calls=%async_computation.15 | async-start | bytes 1310720 | tf_op jit(solution)/shard_map/all_gather | solution.py:28
  868.9 109.8 %all-gather.23.cloned.1.call-start = ((), (), s32[]{:S(2)}) async-start(), calls=%async_computation.8 | async-start | bytes 5242880 | tf_op jit(solution)/shard_map/all_gather | solution.py:28
  869.2 27.9 %copy-start.1 = (bf16[512,2048]{1,0:T(8,128)(2,1)S(1)}, bf16[512,2048]{1,0:T(8,128)(2,1)}, u32[]{:S(2)}) copy-start(bf16[512,2048]{1,0:T(8,128)(2,1)} %get-tuple-element.9) | copy-start | bytes 6291460
Sparse Core Ops, SparseCore 0:
  10.2 10.6 reduce-scatter.4
  23.1 10.7 reduce-scatter.2
  36.1 29.2 all-gather.24
  67.4 80.1 all-gather.12
  153.5 79.3 all-reduce.11
  253.5 25.3 all-gather.26
  281.0 80.1 all-gather.14
  363.3 26.4 all-gather.28
  391.9 80.1 all-gather.16
  478.1 79.3 all-reduce.9
  560.6 28.0 all-gather.30
  590.1 80.1 all-gather.18
  672.4 26.4 all-gather.32
  700.3 80.0 all-gather.20
  786.5 79.3 all-reduce.7
  869.0 28.0 all-gather.34
  898.5 80.1 all-gather.22
where the time goes:
time: 995 us
  waiting for transfers between devices  864 us (87%)
  matrix products  91.9 us (9%)
  between operations  15.6 us (2%)
  blocking collectives  12.3 us (1%)
    all_gather x6, waiting for transfers between devices, second_product(): lax.all_gather(first_half, 'fs', axis=0, tiled=True)  296 us
    psum x3, waiting for transfers between devices, on_device(): lax.psum(local_gram(values[0], columns[0]).astype(jnp.bfloat16), ('tp', '...  238 us
    all_gather x3, waiting for transfers between devices, on_device(): lax.all_gather(values[0], 'fs', axis=0, tiled=True)  236 us
    all_gather x3, waiting for transfers between devices, on_device(): lax.all_gather(values[1], 'fs', axis=0, tiled=True)  69.1 us
    dot_general x12, matrix products, contract(): lax.dot_general(gram, values, (((gram_axis,), (0,)), ((), ())), preferred...  64.4 us
    dot_general x6, matrix products, local_gram(): lax.dot_general(values, columns, (((1,), (1,)), ((), ())), preferred_elem...  27.5 us
  transfers between devices with their start and end apart: 17, of which 17 were waited for; matrix products, arithmetic and copies ran while one was open for 6% of the time, Pallas kernels for 0%

commit v1 on v0

--- a/solution.py
+++ b/solution.py
@@ -53,9 +53,12 @@
             lax.all_gather(values[1], "fs", axis=0, tiled=True),
         )
         gram_sums = (
-            lax.psum(local_gram(values[0], columns[0]).astype(jnp.bfloat16), ("tp", "rep")).astype(
-                jnp.float32
-            ),
+            jnp.sum(
+                lax.all_gather(
+                    local_gram(values[0], columns[0]).astype(jnp.bfloat16), ("tp", "rep")
+                ),
+                axis=0,
+            ).astype(jnp.float32),
             lax.psum(local_gram(values[1], columns[1]).astype(jnp.bfloat16), ("tp", "rep")).astype(
                 jnp.float32
             ),

time: 995 us -> 1210 us (1.22)
  waiting for transfers between devices: 864 us -> 1040 us
  other arithmetic: 9.21 us -> 41.3 us
    all_gather x0 -> x3, waiting for transfers between devices: none -> 264 us  [on_device(): lax.all_gather(local_gram(values[0], columns[0]).astype(jnp.bfloat16), ('...]
    psum x3, waiting for transfers between devices: 238 us -> 173 us  [on_device(): lax.psum(local_gram(values[1], columns[1]).astype(jnp.bfloat16), ('tp', '...]
    reduce_sum x0 -> x4, other arithmetic: none -> 34.4 us  [the longest x3 31.1 us: on_device(): jnp.sum(lax.all_gather(local_gram(values[0], columns[0]).astype(jnp.bfloa...]
    all_gather x6, waiting for transfers between devices: 296 us -> 279 us  [second_product(): lax.all_gather(first_half, 'fs', axis=0, tiled=True)]
  transfers between devices with their start and end apart: 17 -> 20, of which waited for: 17 -> 20; matrix products, arithmetic and copies ran while one was open for 6% -> 9% of each run, Pallas kernels for 0% -> 0%
where the time goes in v1:
time: 1210 us
  waiting for transfers between devices  1040 us (86%)
  matrix products  91.7 us (8%)
  other arithmetic  41.3 us (3%)
  between operations  16 us (1%)
  blocking collectives  12.3 us (1%)
    all_gather x6, waiting for transfers between devices, second_product(): lax.all_gather(first_half, 'fs', axis=0, tiled=True)  279 us
    all_gather x3, waiting for transfers between devices, on_device(): lax.all_gather(local_gram(values[0], columns[0]).astype(jnp.bfloat16), ('...  264 us
    all_gather x3, waiting for transfers between devices, on_device(): lax.all_gather(values[0], 'fs', axis=0, tiled=True)  236 us
    psum x3, waiting for transfers between devices, on_device(): lax.psum(local_gram(values[1], columns[1]).astype(jnp.bfloat16), ('tp', '...  173 us
    all_gather x3, waiting for transfers between devices, on_device(): lax.all_gather(values[1], 'fs', axis=0, tiled=True)  69 us
    dot_general x12, matrix products, contract(): lax.dot_general(gram, values, (((gram_axis,), (0,)), ((), ())), preferred...  64.1 us
    reduce_sum x3, other arithmetic, on_device(): jnp.sum(lax.all_gather(local_gram(values[0], columns[0]).astype(jnp.bfloa...  31.1 us
    dot_general x6, matrix products, local_gram(): lax.dot_general(values, columns, (((1,), (1,)), ((), ())), preferred_elem...  27.6 us
  transfers between devices with their start and end apart: 20, of which 20 were waited for; matrix products, arithmetic and copies ran while one was open for 9% of the time, Pallas kernels for 0%

profile of v1, /device:TPU:0, one launch (start us, length us, event | category | flops | bytes accessed | tf_op | source)
XLA Modules:
  0.0 1207.5 jit_solution(7052504355610226510)
XLA Ops:
  7.2 0.7 reduce-scatter.5.cloned.1.call-update
  8.0 0.7 reduce-scatter.3.cloned.1.call-update
  8.7 12.2 %reduce-scatter.5.cloned.1.call-done = bf16[512,256]{1,0:T(8,128)(2,1)} async-done(((bf16[512,512]{1,0:T(8,128)(2,1)}), bf16[512,256]{1,0:T(8,128)(2,1)}) %reduce-scatter.5.cloned.1.call-update) | async-done | bytes 262160 | tf_op jit(solution)/shard_map/reduce_scatter | solution.py:39
  20.9 1.9 fusion.25
  22.8 0.0 all-gather.19.cloned.1.call-start
  22.9 11.0 reduce-scatter.3.cloned.1.call-done
  33.9 3.3 fusion.26
  37.3 0.0 all-reduce.5.cloned.1.call-start
  37.3 28.1 %all-gather.31.cloned.1.call-done = bf16[2048,256]{1,0:T(8,128)(2,1)} async-done(((bf16[512,256]{1,0:T(8,128)(2,1)}), bf16[2048,256]{1,0:T(8,128)(2,1)}) %all-gather.31.cloned.1.call-update) | async-done | bytes 1048592 | tf_op jit(solution)/shard_map/all_gather | solution.py:53
  65.4 3.3 convolution_convert_fusion.2
  68.7 0.0 all-gather.43.cloned.1.call-start
  68.7 78.8 %all-gather.19.cloned.1.call-done = bf16[2048,1024]{1,0:T(8,128)(2,1)} async-done(((bf16[512,1024]{1,0:T(8,128)(2,1)}), bf16[2048,1024]{1,0:T(8,128)(2,1)}) %all-gather.19.cloned.1.call-update) | async-done | bytes 4194320 | tf_op jit(solution)/shard_map/all_gather | solution.py:52
  147.5 5.9 convolution_convert_fusion.5
  153.4 0.0 all-gather.33.cloned.1.call-start
  153.5 58.0 %all-reduce.5.cloned.1.call-done = bf16[512,2048]{1,0:T(8,128)(2,1)} async-done(((bf16[512,2048]{1,0:T(8,128)(2,1)}), bf16[512,2048]{1,0:T(8,128)(2,1)}) %all-reduce.5.cloned.1.call-update) | async-done | bytes 2097168 | tf_op jit(solution)/shard_map/psum | solution.py:62
  211.4 3.3 fusion.2
  214.7 87.9 %all-gather.43.cloned.1.call-done = bf16[4096,2048]{1,0:T(8,128)(2,1)} async-done(((bf16[512,2048]{1,0:T(8,128)(2,1)}), bf16[4096,2048]{1,0:T(8,128)(2,1)}) %all-gather.43.cloned.1.call-update) | async-done | bytes 16777232 | tf_op jit(solution)/shard_map/all_gather | solution.py:57
  302.6 9.5 reduce_sum.54
  312.1 1.7 fusion
  313.8 12.3 %all-reduce = (f32[]{:T(128)}, f32[]{:T(128)}) all-reduce(f32[]{:T(128)} %fusion, f32[]{:T(128)} %fusion.2), channel_id=1, replica_groups=mesh['fs'=4,'tp'=4,'rep'=2] {'fs'}, use_global_device_ids=true, to_apply=%region_3.0 | all-reduce | flops 2 | bytes 16 | tf_op jit(solution)/shard_map/psum | solution.py:68
  326.8 3.2 fusion.31
  330.0 0.0 all-gather.21.cloned.1.call-start
  330.9 6.3 multiply_convert_fusion
  337.2 0.0 all-gather.35.cloned.1.call-start
  337.2 18.2 %all-gather.33.cloned.1.call-done = bf16[2048,256]{1,0:T(8,128)(2,1)} async-done(((bf16[512,256]{1,0:T(8,128)(2,1)}), bf16[2048,256]{1,0:T(8,128)(2,1)}) %all-gather.33.cloned.1.call-update) | async-done | bytes 1048592 | tf_op jit(solution)/shard_map/all_gather | solution.py:28
  355.4 3.4 fusion.32
  358.9 0.0 all-gather.23.cloned.1.call-start
  359.0 78.8 %all-gather.21.cloned.1.call-done = bf16[2048,1024]{1,0:T(8,128)(2,1)} async-done(((bf16[512,1024]{1,0:T(8,128)(2,1)}), bf16[2048,1024]{1,0:T(8,128)(2,1)}) %all-gather.21.cloned.1.call-update) | async-done | bytes 4194320 | tf_op jit(solution)/shard_map/all_gather | solution.py:28
  437.7 7.5 fusion.27
  445.3 0.2 all-reduce.7.cloned.1.call-start
  445.5 20.8 %all-gather.35.cloned.1.call-done = bf16[2048,256]{1,0:T(8,128)(2,1)} async-done(((bf16[512,256]{1,0:T(8,128)(2,1)}), bf16[2048,256]{1,0:T(8,128)(2,1)}) %all-gather.35.cloned.1.call-update) | async-done | bytes 1048592 | tf_op jit(solution)/shard_map/all_gather | solution.py:53
  466.4 3.3 convolution_convert_fusion.1
  469.7 0.0 all-gather.45.cloned.1.call-start
  469.8 78.7 %all-gather.23.cloned.1.call-done = bf16[2048,1024]{1,0:T(8,128)(2,1)} async-done(((bf16[512,1024]{1,0:T(8,128)(2,1)}), bf16[2048,1024]{1,0:T(8,128)(2,1)}) %all-gather.23.cloned.1.call-update) | async-done | bytes 4194320 | tf_op jit(solution)/shard_map/all_gather | solution.py:52
  548.5 5.9 convolution_convert_fusion.4
  554.4 0.0 all-gather.37.cloned.1.call-start
  554.5 57.6 %all-reduce.7.cloned.1.call-done = bf16[512,2048]{1,0:T(8,128)(2,1)} async-done(((bf16[512,2048]{1,0:T(8,128)(2,1)}), bf16[512,2048]{1,0:T(8,128)(2,1)}) %all-reduce.7.cloned.1.call-update) | async-done | bytes 2097168 | tf_op jit(solution)/shard_map/psum | solution.py:62
  612.0 3.0 fusion.33
  615.0 0.0 all-gather.25.cloned.1.call-start
  615.1 88.1 %all-gather.45.cloned.1.call-done = bf16[4096,2048]{1,0:T(8,128)(2,1)} async-done(((bf16[512,2048]{1,0:T(8,128)(2,1)}), bf16[4096,2048]{1,0:T(8,128)(2,1)}) %all-gather.45.cloned.1.call-update) | async-done | bytes 16777232 | tf_op jit(solution)/shard_map/all_gather | solution.py:57
  703.2 10.8 reduce_sum.56
  714.0 7.0 fusion.28
  721.0 0.0 all-gather.39.cloned.1.call-start
  721.1 12.2 %all-gather.37.cloned.1.call-done = bf16[2048,256]{1,0:T(8,128)(2,1)} async-done(((bf16[512,256]{1,0:T(8,128)(2,1)}), bf16[2048,256]{1,0:T(8,128)(2,1)}) %all-gather.37.cloned.1.call-update) | async-done | bytes 1048592 | tf_op jit(solution)/shard_map/all_gather | solution.py:28
  733.3 2.8 fusion.34
  736.1 0.0 all-gather.27.cloned.1.call-start
  736.2 78.7 %all-gather.25.cloned.1.call-done = bf16[2048,1024]{1,0:T(8,128)(2,1)} async-done(((bf16[512,1024]{1,0:T(8,128)(2,1)}), bf16[2048,1024]{1,0:T(8,128)(2,1)}) %all-gather.25.cloned.1.call-update) | async-done | bytes 4194320 | tf_op jit(solution)/shard_map/all_gather | solution.py:28
  814.9 8.3 fusion.29
  823.3 0.0 all-reduce.9.cloned.1.call-start
  823.3 20.1 %all-gather.39.cloned.1.call-done = bf16[2048,256]{1,0:T(8,128)(2,1)} async-done(((bf16[512,256]{1,0:T(8,128)(2,1)}), bf16[2048,256]{1,0:T(8,128)(2,1)}) %all-gather.39.cloned.1.call-update) | async-done | bytes 1048592 | tf_op jit(solution)/shard_map/all_gather | solution.py:53
  843.4 3.3 convolution_convert_fusion
  846.8 78.2 %all-gather.27.cloned.1.call-done = bf16[2048,1024]{1,0:T(8,128)(2,1)} async-done(((bf16[512,1024]{1,0:T(8,128)(2,1)}), bf16[2048,1024]{1,0:T(8,128)(2,1)}) %all-gather.27.cloned.1.call-update) | async-done | bytes 4194320 | tf_op jit(solution)/shard_map/all_gather | solution.py:52
  925.0 5.9 convolution_convert_fusion.3
  930.9 0.3 all-gather.41.cloned.1.call-start
  931.1 57.2 %all-reduce.9.cloned.1.call-done = bf16[512,2048]{1,0:T(8,128)(2,1)} async-done(((bf16[512,2048]{1,0:T(8,128)(2,1)}), bf16[512,2048]{1,0:T(8,128)(2,1)}) %all-reduce.9.cloned.1.call-update) | async-done | bytes 2097168 | tf_op jit(solution)/shard_map/psum | solution.py:62
  988.3 3.0 fusion.35
  991.3 0.0 all-gather.29.cloned.1.call-start
  991.4 88.1 %all-gather.47.cloned.1.call-done = bf16[4096,2048]{1,0:T(8,128)(2,1)} async-done(((bf16[512,2048]{1,0:T(8,128)(2,1)}), bf16[4096,2048]{1,0:T(8,128)(2,1)}) %all-gather.47.cloned.1.call-update) | async-done | bytes 16777232 | tf_op jit(solution)/shard_map/all_gather | solution.py:57
  1079.5 10.8 reduce_sum.57
  1090.3 7.0 fusion.30
  1097.3 12.3 %all-gather.41.cloned.1.call-done = bf16[2048,256]{1,0:T(8,128)(2,1)} async-done(((bf16[512,256]{1,0:T(8,128)(2,1)}), bf16[2048,256]{1,0:T(8,128)(2,1)}) %all-gather.41.cloned.1.call-update) | async-done | bytes 1048592 | tf_op jit(solution)/shard_map/all_gather | solution.py:28
  1109.6 3.1 broadcast_multiply_fusion.1
  1112.7 78.5 %all-gather.29.cloned.1.call-done = bf16[2048,1024]{1,0:T(8,128)(2,1)} async-done(((bf16[512,1024]{1,0:T(8,128)(2,1)}), bf16[2048,1024]{1,0:T(8,128)(2,1)}) %all-gather.29.cloned.1.call-update) | async-done | bytes 4194320 | tf_op jit(solution)/shard_map/all_gather | solution.py:28
  1191.2 9.5 broadcast_multiply_fusion
  (52 shorter events, 0.5 us)
Async XLA Ops:
  7.2 13.7 %copy-start.12 = (f32[512,256]{1,0:T(8,128)S(1)}, f32[512,256]{1,0:T(8,128)}, u32[]{:S(2)}) copy-start(f32[512,256]{1,0:T(8,128)} %param.10) | copy-start | bytes 1572868
  7.2 13.7 %reduce-scatter.5.cloned.1.call-start = ((), (), s32[]{:S(2)}) async-start(), calls=%async_computation.9 | async-start | bytes 786432 | tf_op jit(solution)/shard_map/reduce_scatter | solution.py:39
  7.9 26.0 %copy-start.7 = (f32[512,1024]{1,0:T(8,128)S(1)}, f32[512,1024]{1,0:T(8,128)}, u32[]{:S(2)}) copy-start(f32[512,1024]{1,0:T(8,128)} %param.7) | copy-start | bytes 6291460
  7.9 26.0 %reduce-scatter.3.cloned.1.call-start = ((), (), s32[]{:S(2)}) async-start(), calls=%async_computation.2 | async-start | bytes 3145728 | tf_op jit(solution)/shard_map/reduce_scatter | solution.py:33
  8.7 56.7 %all-gather.31.cloned.1.call-start = ((), (), s32[]{:S(2)}) async-start(), calls=%async_computation.10 | async-start | bytes 1310720 | tf_op jit(solution)/shard_map/all_gather | solution.py:53
  22.8 42.6 %copy-start.6 = (bf16[512,256]{1,0:T(8,128)(2,1)S(1)}, bf16[512,256]{1,0:T(8,128)(2,1)}, u32[]{:S(2)}) copy-start(bf16[512,256]{1,0:T(8,128)(2,1)} %get-tuple-element.8) | copy-start | bytes 786436
  22.8 124.7 %all-gather.19.cloned.1.call-start = ((), (), s32[]{:S(2)}) async-start(), calls=%async_computation.3 | async-start | bytes 5242880 | tf_op jit(solution)/shard_map/all_gather | solution.py:52
  37.3 110.3 %copy-start.4 = (bf16[512,1024]{1,0:T(8,128)(2,1)S(1)}, bf16[512,1024]{1,0:T(8,128)(2,1)}, u32[]{:S(2)}) copy-start(bf16[512,1024]{1,0:T(8,128)(2,1)} %get-tuple-element.10) | copy-start | bytes 3145732
  37.3 174.2 %all-reduce.5.cloned.1.call-start = ((), (), s32[]{:S(2)}) async-start(), calls=%async_computation.11 | async-start | bytes 4194304 | tf_op jit(solution)/shard_map/psum | solution.py:62
  68.7 233.9 %all-gather.43.cloned.1.call-start = ((), (), s32[]{:S(2)}) async-start(), calls=%async_computation.19 | async-start | bytes 18874368 | tf_op jit(solution)/shard_map/all_gather | solution.py:57
  153.4 202.0 %all-gather.33.cloned.1.call-start = ((), (), s32[]{:S(2)}) async-start(), calls=%async_computation.12 | async-start | bytes 1310720 | tf_op jit(solution)/shard_map/all_gather | solution.py:28
  312.1 14.8 %copy-start.8 = (bf16[2048,256]{1,0:T(8,128)(2,1)S(1)}, bf16[2048,256]{1,0:T(8,128)(2,1)}, u32[]{:S(2)}) copy-start(bf16[2048,256]{1,0:T(8,128)(2,1)} %all-gather.31.cloned.1.call-done) | copy-start | bytes 3145732
  330.0 107.7 %all-gather.21.cloned.1.call-start = ((), (), s32[]{:S(2)}) async-start(), calls=%async_computation.4 | async-start | bytes 5242880 | tf_op jit(solution)/shard_map/all_gather | solution.py:28
  330.9 24.6 %copy-start.13 = (f32[512,256]{1,0:T(8,128)S(1)}, f32[512,256]{1,0:T(8,128)}, u32[]{:S(2)}) copy-start(f32[512,256]{1,0:T(8,128)} %get-tuple-element.9) | copy-start | bytes 1572868
  330.9 24.5 %copy-start.14 = (f32[512,256]{1,0:T(8,128)S(1)}, f32[512,256]{1,0:T(8,128)}, u32[]{:S(2)}) copy-start(f32[512,256]{1,0:T(8,128)} %get-tuple-element.27) | copy-start | bytes 1572868
  337.2 129.2 %all-gather.35.cloned.1.call-start = ((), (), s32[]{:S(2)}) async-start(), calls=%async_computation.13 | async-start | bytes 1310720 | tf_op jit(solution)/shard_map/all_gather | solution.py:53
  358.9 189.6 %all-gather.23.cloned.1.call-start = ((), (), s32[]{:S(2)}) async-start(), calls=%async_computation.5 | async-start | bytes 5242880 | tf_op jit(solution)/shard_map/all_gather | solution.py:52
  437.7 28.7 %copy-start.11 = (bf16[512,256]{1,0:T(8,128)(2,1)S(1)}, bf16[512,256]{1,0:T(8,128)(2,1)}, u32[]{:S(2)}) copy-start(bf16[512,256]{1,0:T(8,128)(2,1)} %get-tuple-element.28) | copy-start | bytes 786436
  445.3 103.2 %copy-start.9 = (bf16[512,1024]{1,0:T(8,128)(2,1)S(1)}, bf16[512,1024]{1,0:T(8,128)(2,1)}, u32[]{:S(2)}) copy-start(bf16[512,1024]{1,0:T(8,128)(2,1)} %get-tuple-element.18) | copy-start | bytes 3145732
  445.3 166.7 %all-reduce.7.cloned.1.call-start = ((), (), s32[]{:S(2)}) async-start(), calls=%async_computation.14 | async-start | bytes 4194304 | tf_op jit(solution)/shard_map/psum | solution.py:62
  469.7 233.4 %all-gather.45.cloned.1.call-start = ((), (), s32[]{:S(2)}) async-start(), calls=%async_computation.20 | async-start | bytes 18874368 | tf_op jit(solution)/shard_map/all_gather | solution.py:57
  554.4 57.6 %copy-start.2 = (bf16[2048,256]{1,0:T(8,128)(2,1)S(1)}, bf16[2048,256]{1,0:T(8,128)(2,1)}, u32[]{:S(2)}) copy-start(bf16[2048,256]{1,0:T(8,128)(2,1)} %all-gather.35.cloned.1.call-done) | copy-start | bytes 3145732
  554.4 178.9 %all-gather.37.cloned.1.call-start = ((), (), s32[]{:S(2)}) async-start(), calls=%async_computation.15 | async-start | bytes 1310720 | tf_op jit(solution)/shard_map/all_gather | solution.py:28
  615.0 199.8 %all-gather.25.cloned.1.call-start = ((), (), s32[]{:S(2)}) async-start(), calls=%async_computation.6 | async-start | bytes 5242880 | tf_op jit(solution)/shard_map/all_gather | solution.py:28
  714.0 19.4 %copy-start = (bf16[512,2048]{1,0:T(8,128)(2,1)S(1)}, bf16[512,2048]{1,0:T(8,128)(2,1)}, u32[]{:S(2)}) copy-start(bf16[512,2048]{1,0:T(8,128)(2,1)} %all-reduce.7.cloned.1.call-done) | copy-start | bytes 6291460
  721.0 122.4 %all-gather.39.cloned.1.call-start = ((), (), s32[]{:S(2)}) async-start(), calls=%async_computation.16 | async-start | bytes 1310720 | tf_op jit(solution)/shard_map/all_gather | solution.py:53
  736.1 188.8 %all-gather.27.cloned.1.call-start = ((), (), s32[]{:S(2)}) async-start(), calls=%async_computation.7 | async-start | bytes 5242880 | tf_op jit(solution)/shard_map/all_gather | solution.py:52
  814.9 28.5 %copy-start.5 = (bf16[512,256]{1,0:T(8,128)(2,1)S(1)}, bf16[512,256]{1,0:T(8,128)(2,1)}, u32[]{:S(2)}) copy-start(bf16[512,256]{1,0:T(8,128)(2,1)} %get-tuple-element.32) | copy-start | bytes 786436
  823.3 101.7 %copy-start.10 = (bf16[512,1024]{1,0:T(8,128)(2,1)S(1)}, bf16[512,1024]{1,0:T(8,128)(2,1)}, u32[]{:S(2)}) copy-start(bf16[512,1024]{1,0:T(8,128)(2,1)} %get-tuple-element.22) | copy-start | bytes 3145732
  823.3 165.0 %all-reduce.9.cloned.1.call-start = ((), (), s32[]{:S(2)}) async-start(), calls=%async_computation.17 | async-start | bytes 4194304 | tf_op jit(solution)/shard_map/psum | solution.py:62
  846.7 232.7 %all-gather.47.cloned.1.call-start = ((), (), s32[]{:S(2)}) async-start(), calls=%async_computation.21 | async-start | bytes 18874368 | tf_op jit(solution)/shard_map/all_gather | solution.py:57
  930.8 57.5 %copy-start.3 = (bf16[2048,256]{1,0:T(8,128)(2,1)S(1)}, bf16[2048,256]{1,0:T(8,128)(2,1)}, u32[]{:S(2)}) copy-start(bf16[2048,256]{1,0:T(8,128)(2,1)} %all-gather.39.cloned.1.call-done) | copy-start | bytes 3145732
  930.9 178.8 %all-gather.41.cloned.1.call-start = ((), (), s32[]{:S(2)}) async-start(), calls=%async_computation.18 | async-start | bytes 1310720 | tf_op jit(solution)/shard_map/all_gather | solution.py:28
  991.3 199.8 %all-gather.29.cloned.1.call-start = ((), (), s32[]{:S(2)}) async-start(), calls=%async_computation.8 | async-start | bytes 5242880 | tf_op jit(solution)/shard_map/all_gather | solution.py:28
  1090.3 19.3 %copy-start.1 = (bf16[512,2048]{1,0:T(8,128)(2,1)S(1)}, bf16[512,2048]{1,0:T(8,128)(2,1)}, u32[]{:S(2)}) copy-start(bf16[512,2048]{1,0:T(8,128)(2,1)} %all-reduce.9.cloned.1.call-done) | copy-start | bytes 6291460
Sparse Core Ops, SparseCore 0:
  10.2 10.6 reduce-scatter.4
  23.1 10.7 reduce-scatter.2
  36.1 29.2 all-gather.30
  67.4 80.1 all-gather.18
  151.2 60.2 all-reduce.4
  213.8 88.7 all-gather.42
  330.2 25.2 all-gather.32
  357.6 80.1 all-gather.20
  439.9 26.4 all-gather.34
  468.3 80.1 all-gather.22
  551.7 60.2 all-reduce.6
  614.3 88.7 all-gather.44
  705.3 27.9 all-gather.36
  734.7 80.1 all-gather.24
  816.9 26.4 all-gather.38
  844.8 80.1 all-gather.26
  928.0 60.2 all-reduce.8
  990.6 88.7 all-gather.46
  1081.6 27.9 all-gather.40
  1111.0 80.1 all-gather.28
